TPU v7x, 512 devices: a 4x2x32 block of a 4x8x32 slice. The times are simulated.
512 devices in a mesh: grp: 2 (over y), sp: 64 (over z, core), tp: 4 (over x).
Axes of the slice: x: 4, y: 2, z: 32, core: 2. Of those that a mesh axis runs over, the one named last changes fastest.
The devices are a block of a 4x8x32 slice.
Arguments:
- tokens: bfloat16 [16384, 2048], P(('grp', 'sp'), 'tp'), parts along dimension 0, may hold values from -6 to 6
- norm_gain: float32 [2048], replicated, may hold values from 0.1 to 1.9
- att_q_weight: bfloat16 [1024, 2048], P('tp', 'sp'), may hold values from -0.625 to 0.625
- att_k_weight: bfloat16 [512, 2048], P('tp', 'sp'), may hold values from -0.125 to 0.125
- att_v_weight: bfloat16 [512, 2048], P('tp', 'sp'), may hold values from -0.125 to 0.125
- rec_q_weight: bfloat16 [1024, 2048], P('tp', 'sp'), may hold values from -0.125 to 0.125
- rec_f_weight: bfloat16 [1024, 2048], P('tp', 'sp'), may hold values from -0.125 to 0.125
- rec_i_weight: bfloat16 [1024, 2048], P('tp', 'sp'), may hold values from -0.125 to 0.125
- att_out_weight: bfloat16 [1024, 2048], P('tp', 'sp'), may hold values from -1.5 to 1.5
- rec_out_weight: bfloat16 [1024, 2048], P('tp', 'sp'), may hold values from -0.1875 to 0.1875
- score_offset: float32 [16], P('tp'), may hold values from -11.5 to -3
- lower_bound: float32 [1024], P('tp'), may hold values from 0.94 to 0.99999
- decay_shift: float32 [16384, 1024], P(('grp', 'sp'), 'tp'), parts along dimension 0, may hold values from -2.1 to 0
- rec_gain: float32 [1024], P('tp'), may hold values from 0.1 to 1.9
Outputs:
- mixed: bfloat16 [16384, 2048], P(('grp', 'sp', 'tp')), parts along dimension 0
There are 2 independent parts, one for each index of `grp`. A program takes and returns all parts, laid end to end along the dimension named above; an argument that names none is the same for every part. Nothing has to cross between parts.
All inputs are finite; a program needn't handle non-finite values.
Results may differ from a plain program's by a relative error of at most 0.015.
Values may be sent and summed in bfloat16 or wider, within the bound.
A program may use at most 64 MiB of HBM per device.

v0:
```python
import jax
import jax.numpy as jnp
from jax import lax
from jax.sharding import PartitionSpec as P

HEAD = 64
REC_KEY = 128
REC_VAL = 128
SPAN = 64


EPS = 1e-06


def from_everyone(x, axis):
    count = lax.axis_size(axis)
    return lax.all_to_all(jnp.broadcast_to(x[None], (count, *x.shape)), axis, 0, 0, tiled=True)


def in_order(tiles, dim):
    shape = list(tiles.shape[1:])
    shape[dim] *= tiles.shape[0]
    return jnp.moveaxis(tiles, 0, dim).reshape(shape)


def gathered_copies(x, axis, dim):
    tiles = from_everyone(x, axis)
    return in_order(tiles, dim)


def entering(x, axis, combine, identity):
    count, here = (lax.axis_size(axis), lax.axis_index(axis))
    everything = jax.tree.map(
        lambda part, kind: lax.all_gather(part.astype(kind), axis), x, (jnp.bfloat16, jnp.bfloat16)
    )
    start = jax.tree.map(
        lambda part, zero: jnp.broadcast_to(jnp.asarray(zero, part.dtype), part.shape), x, identity
    )

    def entering_turn(k, before):
        reached = k < here
        new = combine(
            before, jax.tree.map(lambda part, own: part[k].astype(own.dtype), everything, x)
        )
        return jax.tree.map(lambda a, b: jnp.where(reached, a, b), new, before)

    return lax.fori_loop(0, count, entering_turn, start)


def gather_turned(arrays, axis, dims):
    turned = [jnp.moveaxis(a, dim, 0) for a, dim in zip(arrays, dims)]
    both = jnp.concatenate([t.reshape(len(t), -1) for t in turned], axis=1)
    result, at, done = (lax.all_gather(both, axis, axis=0, tiled=True), 0, [])
    for t, dim in zip(turned, dims):
        share = result[:, at : at + t[0].size].reshape(-1, *t.shape[1:])
        done.append(jnp.moveaxis(share, 0, dim))
        at += t[0].size
    return tuple(done)


def cut_along(x, dim, count):
    before, after = (x.shape[:dim], x.shape[dim + 1 :])
    return jnp.moveaxis(x.reshape(*before, count, -1, *after), dim, 0)


def sum_at_owner(x, axis, dim):
    count = lax.axis_size(axis)
    tiles = lax.all_to_all(cut_along(x, dim, count), axis, 0, 0, tiled=True)
    return jnp.sum(tiles.astype(jnp.float32), axis=0)


def make_fold(norm_gain, weights, carry, piece):
    elementwise_sq, totals = carry
    raw = piece.astype(jnp.float32)
    scaled = (raw * norm_gain[None, :]).astype(jnp.bfloat16)
    elementwise_sq = jnp.sum(raw * raw, axis=1)
    updated = []
    for total, weight in zip(totals, weights):
        updated.append(
            lax.dot_general(
                scaled, weight, (((1,), (1,)), ((), ())), preferred_element_type=jnp.float32
            )
        )
    return (elementwise_sq, tuple(updated))


def project_all(tokens, norm_gain, weights):
    rows = tokens.shape[0]
    width = weights[0].shape[1]
    start_carry = (
        jnp.zeros((rows,), jnp.float32),
        tuple((jnp.zeros((rows, weight.shape[0]), jnp.float32) for weight in weights)),
    )
    elementwise_sq, totals = make_fold(
        norm_gain, weights, start_carry, gathered_copies(tokens, "tp", 1)
    )
    inv_rms = lax.rsqrt(elementwise_sq / width + EPS)
    return tuple((total * inv_rms[:, None] for total in totals))


def attention(att_query, key_value, score_offset):
    rows = att_query.shape[0]
    gathered = lax.all_gather(key_value, "sp", axis=0, tiled=True)
    seq = gathered.shape[0]
    kv_heads = key_value.shape[1] // (2 * HEAD)
    q_heads = att_query.shape[1] // HEAD
    group = q_heads // kv_heads
    kv_width = kv_heads * HEAD
    queries = att_query.reshape(rows, kv_heads, group, HEAD)
    offsets = score_offset.reshape(kv_heads, group)
    kblock = min(1024, seq)
    first_row = lax.axis_index("sp") * rows
    query_pos = first_row + jnp.arange(rows, dtype=jnp.int32)
    count = (first_row + rows - 1) // kblock + 1

    def attention_turn(step, carry):
        summed, run = carry
        block_start = (count - 1 - step) * kblock
        block = lax.dynamic_slice_in_dim(gathered, block_start, kblock, 0)
        keys = block[:, :kv_width].reshape(kblock, kv_heads, HEAD)
        values = block[:, kv_width:].reshape(kblock, kv_heads, HEAD)
        score = (
            jnp.einsum("tkgd,skd->tkgs", queries, keys, preferred_element_type=jnp.float32)
            * HEAD ** (-0.5)
            + offsets[None, :, :, None]
        )
        key_pos = block_start + jnp.arange(kblock, dtype=jnp.int32)
        visible = (key_pos[None, :] < query_pos[:, None])[:, None, None, :]
        keep = jnp.where(visible, jax.nn.log_sigmoid(-score), 0.0)
        tail = lax.cumsum(keep, axis=3, reverse=True) - keep
        weight = jnp.where(
            visible, jnp.exp(jax.nn.log_sigmoid(score) + tail + run[..., None]), 0.0
        ).astype(jnp.bfloat16)
        summed = summed + jnp.einsum(
            "tkgs,skd->tkgd", weight, values, preferred_element_type=jnp.float32
        )
        return (summed, run + jnp.sum(keep, axis=3))

    start_carry = (
        jnp.zeros((rows, kv_heads, group, HEAD), jnp.float32),
        jnp.zeros((rows, kv_heads, group), jnp.float32),
    )
    summed, _ = lax.fori_loop(0, count, attention_turn, start_carry)
    return summed.reshape(rows, q_heads * HEAD).astype(jnp.bfloat16)


def block_pass(carry, inputs):
    state_matrix, prefix = carry
    query_rows, log_decay, keyed_values, value_rows = inputs
    span = query_rows.shape[0]
    cumulative_log = jnp.cumsum(log_decay, axis=0)
    lower = jnp.arange(span, dtype=jnp.int32)[:, None] >= jnp.arange(span, dtype=jnp.int32)[None, :]
    diff = cumulative_log[:, None] - cumulative_log[None, :]
    decay = jnp.exp(jnp.where(lower[:, :, None, None], diff, -jnp.inf))
    score = jnp.einsum("thk,tshk,shk->ths", query_rows, decay, keyed_values)
    inner = jnp.einsum("ths,shv->thv", score, value_rows)
    outer_product = jnp.einsum("ril,ilc->ric", query_rows * jnp.exp(cumulative_log), state_matrix)
    final_state = cumulative_log[-1]
    state_matrix = state_matrix * jnp.exp(final_state)[:, :, None] + jnp.einsum(
        "iag,iax->agx", keyed_values * jnp.exp(final_state[None] - cumulative_log), value_rows
    )
    reach_limit = query_rows * jnp.exp(cumulative_log + prefix[None])
    return ((state_matrix, prefix + final_state), (inner + outer_product, reach_limit))


def chain(earlier, later):
    return (earlier[0] * later[0], earlier[1] * later[0][:, :, None] + later[1])


def recurrence(rec_query, rec_forget, rec_input, lower_bound, decay_shift, rec_gain):
    rows = rec_query.shape[0]
    heads = rec_gain.shape[0] // REC_VAL
    logit = rec_forget.astype(jnp.float32)
    gap = 1.0 - lower_bound
    log_decay = jnp.log(lower_bound + gap * jax.nn.sigmoid(logit)) + decay_shift
    keyed_values = gap * jax.nn.sigmoid(-logit)
    query_rows = jax.nn.silu(rec_query.astype(jnp.float32))
    blocks = rows // SPAN

    def split(array, depth):
        return array.reshape(blocks, SPAN, heads, depth)

    start_carry = (
        jnp.zeros((heads, REC_KEY, REC_VAL), jnp.float32),
        jnp.zeros((heads, REC_KEY), jnp.float32),
    )
    (state_matrix, total), (local, reach_limit) = lax.scan(
        block_pass,
        start_carry,
        (
            split(query_rows, REC_KEY),
            split(log_decay, REC_KEY),
            split(keyed_values, REC_KEY),
            split(rec_input.astype(jnp.float32), REC_VAL),
        ),
    )
    identity = (
        jnp.ones((heads, REC_KEY), jnp.float32),
        jnp.zeros((heads, REC_KEY, REC_VAL), jnp.float32),
    )
    incoming_state = entering((jnp.exp(total), state_matrix), "sp", chain, identity)
    running_memory = jnp.einsum("lida,dao->lido", reach_limit, incoming_state[1])
    rec_raw = (local + running_memory).reshape(rows, heads, REC_VAL)
    rescaled_input = (
        rec_raw
        * lax.rsqrt(jnp.mean(rec_raw * rec_raw, axis=2, keepdims=True) + EPS)
        * rec_gain.reshape(heads, REC_VAL)
    )
    return rescaled_input.reshape(rows, heads * REC_VAL).astype(jnp.bfloat16)


def on_device(
    tokens,
    norm_gain,
    att_q_weight,
    att_k_weight,
    att_v_weight,
    rec_q_weight,
    rec_f_weight,
    rec_i_weight,
    att_out_weight,
    rec_out_weight,
    score_offset,
    lower_bound,
    decay_shift,
    rec_gain,
):
    gathered = gather_turned(
        (
            att_q_weight,
            att_k_weight,
            att_v_weight,
            rec_q_weight,
            rec_f_weight,
            rec_i_weight,
            att_out_weight,
            rec_out_weight,
        ),
        "sp",
        (1, 1, 1, 1, 1, 1, 1, 1),
    )
    inputs = gathered[:6]
    outputs = gathered[6:]
    projected = project_all(tokens, norm_gain, inputs)
    att_query = projected[0].astype(jnp.bfloat16)
    key_value = jnp.concatenate(projected[1:3], axis=1).astype(jnp.bfloat16)
    rec_query = projected[3].astype(jnp.bfloat16)
    rec_forget = projected[4].astype(jnp.bfloat16)
    rec_input = projected[5].astype(jnp.bfloat16)
    att_out = attention(att_query, key_value, score_offset)
    rec_out = recurrence(rec_query, rec_forget, rec_input, lower_bound, decay_shift, rec_gain)
    att_rows, rec_rows = outputs
    return sum_at_owner(
        (
            jnp.dot(att_out, att_rows, preferred_element_type=jnp.float32)
            + jnp.dot(rec_out, rec_rows, preferred_element_type=jnp.float32)
        ).astype(jnp.bfloat16),
        "tp",
        0,
    ).astype(jnp.bfloat16)


def solution(mesh):
    in_specs = (
        P(("grp", "sp"), "tp"),
        P(),
        P("tp", "sp"),
        P("tp", "sp"),
        P("tp", "sp"),
        P("tp", "sp"),
        P("tp", "sp"),
        P("tp", "sp"),
        P("tp", "sp"),
        P("tp", "sp"),
        P("tp"),
        P("tp"),
        P(("grp", "sp"), "tp"),
        P("tp"),
    )
    out_specs = P(("grp", "sp", "tp"), None)
    return jax.shard_map(
        on_device, mesh=mesh, in_specs=in_specs, out_specs=out_specs, check_vma=False
    )
```

profile of v0, /device:TPU:1824, one launch (start us, length us, event | category | flops | bytes accessed | tf_op | source)
XLA Modules:
  0.0 568.7 jit_solution(13439887807807666667)
XLA Ops:
  14.9 4.6 all-to-all-start
  19.5 9.5 %all-to-all-done = bf16[4,128,512]{1,2,0:T(8,128)(2,1)S(1)} async-done(((bf16[4,128,512]{1,2,0:T(8,128)(2,1)}), bf16[4,128,512]{1,2,0:T(8,128)(2,1)S(1)}, u32[]{:S(2)}, u32[]{:S(2)}) %all-to-all-start) | async-done | bytes 524320 | tf_op jit(solution)/shard_map/all_to_all | solution.py:17
  29.7 108.8 %all-gather.7.cloned.1.call-done = bf16[2048,1792]{1,0:T(8,128)(2,1)} async-done(((bf16[32,1792]{1,0:T(8,128)(2,1)}), bf16[2048,1792]{1,0:T(8,128)(2,1)}) %all-gather.7.cloned.1.call-update) | async-done | bytes 7340048 | tf_op jit(solution)/shard_map/all_gather | solution.py:53
  143.6 16.8 %while.47 = (s32[]{:T(128)}, f32[2,128,128]{2,1,0:T(8,128)S(1)}, f32[2,128]{1,0:T(2,128)S(1)}, f32[2,64,2,128]{3,1,0,2:T(8,128)S(1)}, bf16[2,64,2,128]{3,1,0,2:T...) while((s32[]{:T(128)}, f32[2,128,128]{2,1,0:T(8,128)S(1)}, ...), condition=%wide.region_8.9_spmd.clone, body=%wide.region_6.8_spmd.clone.sunk | while | flops 18092548 | bytes 5982349 | solution.py:187
  143.9 6.3 %multiply_bitcast_fusion.2 = bf16[64,2,128,64]{2,1,0,3:T(2,128)(2,1)S(1)} fusion(pred[64,64]{1,0:T(8,128)(4,1)S(1)} %iota_compare_fusion.2, f32[64,2,128]{2,1,0:T(2,128)S(1)} %get-tuple-element.589, f32[64,2,128]{2,1,0:T(2,128)S(1)} %fusion.120), kind=kLoop, calls=%fused_computation.33.clone.1 | loop fusion | flops 4194304 | bytes 2232320 | tf_op jit(solution)/shard_map/while/body/eval_jaxpr/thk,tshk,shk->ths/dot_general | solution.py:155
  152.3 6.3 %multiply_bitcast_fusion.2 = bf16[64,2,128,64]{2,1,0,3:T(2,128)(2,1)S(1)} fusion(pred[64,64]{1,0:T(8,128)(4,1)S(1)} %iota_compare_fusion.2, f32[64,2,128]{2,1,0:T(2,128)S(1)} %get-tuple-element.589, f32[64,2,128]{2,1,0:T(2,128)S(1)} %fusion.120), kind=kLoop, calls=%fused_computation.33.clone.1 | loop fusion | flops 4194304 | bytes 2232320 | tf_op jit(solution)/shard_map/while/body/eval_jaxpr/thk,tshk,shk->ths/dot_general | solution.py:155
  162.9 54.0 %all-gather.2 = bf16[64,2,128]{2,1,0:T(2,128)(2,1)S(1)} all-gather(bf16[1,2,128]{2,1,0:T(2,128)(2,1)S(1)} %fusion.66), channel_id=2, replica_groups=mesh['grp'=2,'sp'=64,'tp'=4] {'sp'}, dimensions={0}, use_global_device_ids=true | all-gather | bytes 33280 | tf_op jit(solution)/shard_map/all_gather | solution.py:34
  220.5 68.8 %all-gather.11.cloned.1.call-done = bf16[128,128,128]{2,1,0:T(8,128)(2,1)} async-done(((bf16[2,128,128]{2,1,0:T(8,128)(2,1)}), bf16[128,128,128]{2,1,0:T(8,128)(2,1)}) %all-gather.11.cloned.1.call-update) | async-done | bytes 4194320 | tf_op jit(solution)/shard_map/all_gather | solution.py:34
  289.2 64.9 %while.48 = (s32[]{:T(128)}, f32[2,128,128]{2,1,0:T(8,128)S(1)}, s32[]{:T(128)}, bf16[64,2,128]{2,1,0:T(2,128)(2,1)S(1)}, bf16[64,2,128,128]{3,2,1,0:T(8,128)(2,1)}, /*index=5*/s32[]{:T(128)}, s32[]{:T(128)}) while((s32[]{:T(128)}, f32[2,128,128]{2,1,0:T(8,128)S(1)}, s32[]{:T(128)}, bf16[64,2,128]{2,1,0:T(2,128)(2,1)S(1)}, ...), condition=%wide.region_10.11_spmd.clone, body=%wide.region_9.10_spmd.clone.sunk | while | flops 164100 | bytes 330345 | solution.py:47
  354.7 69.5 %all-gather.9.cloned.1.call-done = bf16[8192,256]{0,1:T(8,128)(2,1)} async-done(((bf16[128,256]{0,1:T(8,128)(2,1)}), bf16[8192,256]{0,1:T(8,128)(2,1)}) %all-gather.9.cloned.1.call-update) | async-done | bytes 4194320 | tf_op jit(solution)/shard_map/all_gather | solution.py:103
  424.2 119.4 %while.46 = (s32[]{:T(128)}, f32[128,2,2,64]{0,3,2,1:T(8,128)S(1)}, f32[128,2,2]{0,2,1:T(2,128)S(1)}, s32[]{:T(128)}, s32[]{:T(128)}, /*index=5*/bf16[8192,256]{...) while((s32[]{:T(128)}, f32[128,2,2,64]{0,3,2,1:T(8,128)S(1)}, ...), condition=%wide.region_5.6_spmd.clone, body=%wide.region_1.5_spmd.clone.sunk | while | flops 219349632 | bytes 33887552 | solution.py:143
  425.8 3.1 fusion.109
  428.8 5.0 fusion.110
  435.8 3.2 fusion.111
  440.7 3.1 fusion.109
  443.7 5.0 fusion.110
  450.7 3.2 fusion.111
  455.6 3.1 fusion.109
  458.7 5.0 fusion.110
  465.6 3.2 fusion.111
  473.6 5.0 fusion.110
  480.5 3.2 fusion.111
  488.5 5.0 fusion.110
  495.4 3.2 fusion.111
  503.4 5.0 fusion.110
  510.3 3.2 fusion.111
  515.2 3.1 fusion.109
  518.3 5.0 fusion.110
  525.2 3.2 fusion.111
  533.2 5.0 fusion.110
  540.1 3.2 fusion.111
  547.3 14.1 %all_to_all.10 = bf16[4,32,2048]{2,1,0:T(8,128)(2,1)S(1)} all-to-all(bf16[4,32,2048]{2,1,0:T(8,128)(2,1)S(1)} %bitcast.218), channel_id=1, replica_groups=mesh['grp'=2,'sp'=64,'tp'=4] {'tp'}, dimensions={0} | all-to-all | bytes 1048576 | tf_op jit(solution)/shard_map/all_to_all | solution.py:68
  (329 shorter events, 132.1 us)
Async XLA Ops:
  6.5 13.0 %copy-start.4 = (f32[256]{0:T(256)S(1)}, f32[256]{0:T(256)}, u32[]{:S(2)}) copy-start(f32[256]{0:T(256)} %param.31) | copy-start | bytes 3076
  6.5 22.8 %copy-start.2 = (f32[2048]{0:T(1024)S(1)}, f32[2048]{0:T(1024)}, u32[]{:S(2)}) copy-start(f32[2048]{0:T(1024)} %param.21) | copy-start | bytes 24580
  6.6 131.9 %copy-start.5 = (f32[128,256]{1,0:T(8,128)S(1)}, f32[128,256]{1,0:T(8,128)}, u32[]{:S(2)}) copy-start(f32[128,256]{1,0:T(8,128)} %param.32) | copy-start | bytes 393220
  6.6 131.9 %all-gather.7.cloned.1.call-start = ((), (), s32[]{:S(2)}) async-start(), calls=%async_computation.2 | async-start | bytes 7454720 | tf_op jit(solution)/shard_map/all_gather | solution.py:53
  12.3 0.6 copy-start.1
  14.9 14.1 %all-to-all-start = ((bf16[4,128,512]{1,2,0:T(8,128)(2,1)}), bf16[4,128,512]{1,2,0:T(8,128)(2,1)S(1)}, u32[]{:S(2)}, u32[]{:S(2)}) async-start(bf16[4,128,512]{1,2,0:T(8,128)(2,1)} %broadcast_in_dim.57), calls=%async_computation | async-start | bytes 1048576 | tf_op jit(solution)/shard_map/all_to_all | solution.py:17
  19.5 269.8 %all-gather.11.cloned.1.call-start = ((), (), s32[]{:S(2)}) async-start(), calls=%async_computation.4 | async-start | bytes 4259840 | tf_op jit(solution)/shard_map/all_gather | solution.py:34
  161.1 263.0 %all-gather.9.cloned.1.call-start = ((), (), s32[]{:S(2)}) async-start(), calls=%async_computation.3 | async-start | bytes 4259840 | tf_op jit(solution)/shard_map/all_gather | solution.py:103
  218.4 205.8 %copy-start.6 = (f32[4]{0:T(128)S(1)}, f32[4]{0:T(128)}, u32[]{:S(2)}) copy-start(f32[4]{0:T(128)} %param.30) | copy-start | bytes 52
  434.2 1.6 copy-start
  449.1 1.6 copy-start
  464.0 1.6 copy-start
  478.9 1.6 copy-start
  493.8 1.6 copy-start
  508.7 1.6 copy-start
  523.6 1.6 copy-start
  538.5 1.6 copy-start
  543.6 1.9 copy-start.3
Sparse Core Ops, SparseCore 0:
  13.1 125.3 all-gather.6
  161.2 127.9 all-gather.10
  291.3 132.7 all-gather.8
where the time goes:
time: 573 us; the launch traced here: 569 us
  waiting for transfers between devices  257 us (45%)
  other arithmetic  148 us (26%)
  blocking collectives  68.2 us (12%)
  matrix products  43.1 us (8%)
  local copies, waits for them, and re-layouts  31 us (5%)
  between operations  13.4 us (2%)
    all_gather x1, waiting for transfers between devices, gather_turned(): result, at, done = (lax.all_gather(both, axis, axis=0, tiled=True), 0, [])  109 us
    all_gather x1, waiting for transfers between devices, attention(): gathered = lax.all_gather(key_value, 'sp', axis=0, tiled=True)  69.5 us
    all_gather x1, waiting for transfers between devices, entering(): lax.all_gather(part.astype(kind), axis)  68.8 us
    select_n x64, other arithmetic, entering_turn(): return jax.tree.map(lambda a, b: jnp.where(reached, a, b), new, before)  62.1 us
    all_gather x1, blocking collectives, entering(): lax.all_gather(part.astype(kind), axis)  54 us
    another operation x18, other arithmetic  40.6 us
    convert_element_type x8, other arithmetic, attention_turn(): weight = jnp.where(visible, jnp.exp(jax.nn.log_sigmoid(score) + tail + ru...  25.2 us
    dot_general x8, matrix products, attention_turn(): jnp.einsum('tkgd,skd->tkgs', queries, keys, preferred_element_type=jnp.fl...  24.4 us
  transfers between devices with their start and end apart: 4, of which 4 were waited for; matrix products, arithmetic and copies ran while one was open for 12% of the time, Pallas kernels for 0%

commit v1 on v0

v1 whole, which is shorter than its diff:
```python
import functools

import jax
import jax.numpy as jnp
from jax import lax
from jax.experimental import pallas as pl
from jax.experimental.pallas import tpu as pltpu
from jax.sharding import PartitionSpec as P

HEAD = 64
REC = 128
EPS = 1e-06
LOG2E = 1.4426950408889634
MESH = pl.DeviceIdType.MESH
F32 = jnp.float32
BF16 = jnp.bfloat16

PARTS = 4
KV_PARTS = 5
DECAY_ROWS = 16


def nt(a, b):
    return lax.dot_general(a, b, (((1,), (1,)), ((), ())), preferred_element_type=F32)


def nn(a, b):
    return lax.dot_general(a, b, (((1,), (0,)), ((), ())), preferred_element_type=F32)


def iota(shape, dim):
    return lax.broadcasted_iota(jnp.int32, shape, dim)


def greet(devices):
    barrier = pltpu.get_barrier_semaphore()
    for device in devices:
        pl.semaphore_signal(barrier, inc=1, device_id=device, device_id_type=MESH)
    pl.semaphore_wait(barrier, len(devices))


def place(nz):
    sp = lax.axis_index("sp")
    z, c = sp // 2, sp % 2
    partner = {"sp": 2 * z + 1 - c}
    up = {"sp": 2 * ((z + 1) % nz) + c}
    down = {"sp": 2 * ((z + nz - 1) % nz) + c}
    return z, c, partner, up, down


def send(src, dst, send_sem, recv_sem, device):
    return pltpu.make_async_remote_copy(
        src_ref=src,
        dst_ref=dst,
        send_sem=send_sem,
        recv_sem=recv_sem,
        device_id=device,
        device_id_type=MESH,
    )


def gather_kernel(
    nz, ntp, tok, wt, shift, xg, w, shift_out,
    ring_send, ring_recv, swap_send, swap_recv, tok_send, tok_recv,
    relay_send, relay_recv, shift_send, shift_recv, local_sem,
):
    z, c, partner, up, down = place(nz)
    x = lax.axis_index("tp")
    ways = ((up, 0, nz // 2, -1), (down, 1, nz - 1 - nz // 2, 1))
    half = PARTS // 2
    greet([partner, up, down] + [{"tp": (x + i) % ntp} for i in range(1, ntp)])

    locals_, swaps, toks, relays = [], [], [], []
    for p in range(half):
        swaps.append(
            send(wt.at[1 - c, p], w.at[z, half * c + p], swap_send.at[p], swap_recv.at[p], partner)
        )
        locals_.append(
            pltpu.make_async_copy(wt.at[c, p], w.at[z, half * c + p], local_sem.at[p])
        )
    for swap in swaps:
        swap.start()
    first = []
    for p in range(half):
        j = half * c + p
        for device, way, count, _ in ways:
            if count > 0:
                first.append(
                    send(wt.at[c, p], w.at[z, j], ring_send.at[way, 0, j], ring_recv.at[way, 0, j], device)
                )
                first[-1].start()
    for i in range(1, ntp):
        toks.append(
            send(tok, xg.at[x, c], tok_send.at[i - 1], tok_recv.at[i - 1], {"tp": (x + i) % ntp})
        )
        toks[-1].start()
    for p in range(half):
        j = half * (1 - c) + p
        swaps[p].wait_recv()
        for device, way, count, _ in ways:
            if count > 0:
                first.append(
                    send(w.at[z, j], w.at[z, j], ring_send.at[way, 0, j], ring_recv.at[way, 0, j], device)
                )
                first[-1].start()
    relays.append(send(tok, xg.at[x, c], relay_send.at[0], relay_recv.at[0], partner))
    relays[-1].start()
    own = pl.ds(pl.multiple_of(REC * c, REC), REC)
    other = pl.ds(pl.multiple_of(REC * (1 - c), REC), REC)
    shift_copy = send(shift.at[:, other], shift_out.at[c], shift_send, shift_recv, partner)
    shift_copy.start()
    locals_.append(pltpu.make_async_copy(tok, xg.at[x, c], local_sem.at[half]))
    locals_.append(pltpu.make_async_copy(shift.at[:, own], shift_out.at[c], local_sem.at[half + 1]))
    for copy in locals_:
        copy.start()

    def hop(way, d, j, device, sign):
        slot = (z + sign * (d - 1) + nz) % nz
        ref = w.at[slot, j]
        return send(ref, ref, ring_send.at[way, d - 1, j], ring_recv.at[way, d - 1, j], device)

    def arrived(way, d, j, device, sign):
        ref = w.at[(z + sign * d + nz) % nz, j]
        send(ref, ref, ring_send.at[way, d - 1, j], ring_recv.at[way, d - 1, j], device).wait_recv()

    def forward(d, some):
        for j in range(PARTS):
            for device, way, _, sign in some:
                arrived(way, d - 1, j, device, sign)
                hop(way, d, j, device, sign).start()

    def body(d, _):
        forward(d, ways)
        return 0

    both = min(count for _, _, count, _ in ways)
    middle = max(min(both + 1, 6), 2)
    lax.fori_loop(2, middle, body, 0)
    for i in range(1, ntp):
        toks[i - 1].wait_recv()
        ref = xg.at[(x + ntp - i) % ntp, c]
        relays.append(send(ref, ref, relay_send.at[i], relay_recv.at[i], partner))
        relays[-1].start()
    lax.fori_loop(middle, both + 1, body, 0)
    for d in range(both + 1, ways[0][2] + 1):
        if d > 1:
            forward(d, ways[:1])
    for device, way, count, sign in ways:
        for j in range(PARTS):
            if count > 0:
                arrived(way, count, j, device, sign)

    def drain(d, _):
        for j in range(PARTS):
            for device, way, _, sign in ways:
                hop(way, d, j, device, sign).wait_send()
        return 0

    for copy in first:
        copy.wait_send()
    lax.fori_loop(2, both + 1, drain, 0)
    for d in range(max(both + 1, 2), ways[0][2] + 1):
        for j in range(PARTS):
            hop(0, d, j, up, -1).wait_send()
    for copy in swaps + toks:
        copy.wait_send()
    for copy in relays:
        copy.wait()
    shift_copy.wait()
    for copy in locals_:
        copy.wait()


def gather(nz, ntp, tokens, wt, shift):
    rows, width = tokens.shape
    cols = wt.shape[-1]
    steps = nz // 2
    dma = pltpu.SemaphoreType.DMA
    vmem = pl.BlockSpec(memory_space=pltpu.VMEM)
    return pl.pallas_call(
        functools.partial(gather_kernel, nz, ntp),
        out_shape=(
            jax.ShapeDtypeStruct((ntp, 2, rows, width), BF16),
            jax.ShapeDtypeStruct((nz, PARTS, wt.shape[2], cols), BF16),
            jax.ShapeDtypeStruct((2, rows, REC), F32),
        ),
        in_specs=[vmem] * 3,
        out_specs=(vmem,) * 3,
        scratch_shapes=[
            dma((2, steps, PARTS)), dma((2, steps, PARTS)),
            dma((PARTS // 2,)), dma((PARTS // 2,)),
            dma((ntp - 1,)), dma((ntp - 1,)),
            dma((ntp,)), dma((ntp,)),
            dma, dma, dma((PARTS // 2 + 2,)),
        ],
        compiler_params=pltpu.CompilerParams(collective_id=0, has_side_effects=True),
        name="gather_weights",
    )(tokens, wt, shift)


def split3(a):
    hi = a.astype(BF16)
    rest = a - hi.astype(F32)
    mid = rest.astype(BF16)
    low = (rest - mid.astype(F32)).astype(BF16)
    return hi, mid, low


def project_kernel(
    ntp, xg, gain, w, lower, shift, q2, chunk, reach, inner, wv, sem
):
    rows = 2 * xg.shape[2]
    width = xg.shape[3]
    skip = 2 * REC
    copy = pltpu.make_async_copy(w.at[:, :, :, skip:], wv, sem)
    copy.start()
    sq = jnp.zeros((rows, 1), F32)
    scaled = []
    for i in range(ntp):
        raw = xg[i].reshape(rows, width).astype(F32)
        sq = sq + jnp.sum(raw * raw, axis=1, keepdims=True)
        scaled.append((raw * gain[:, i * width : (i + 1) * width]).astype(BF16))
    inv = lax.rsqrt(sq / (ntp * width) + EPS)
    copy.wait()
    per = wv.shape[0] // ntp
    total = None
    for i in range(ntp):
        part = nn(scaled[i], wv[i * per : (i + 1) * per].reshape(width, wv.shape[3]))
        total = part if total is None else total + part
    total = (total * inv).astype(BF16)
    lane = iota((rows, REC), 1)
    q = total[:, :REC].astype(F32)
    q2[0:rows] = jnp.where(lane < HEAD, q, 0.0).astype(BF16)
    q2[rows : 2 * rows] = jnp.where(lane < HEAD, pltpu.roll(q, HEAD, 1), 0.0).astype(BF16)
    chunk[0:rows] = total[:, REC : 2 * REC]
    rq = total[:, 2 * REC : 3 * REC].astype(F32)
    logit = total[:, 3 * REC : 4 * REC].astype(F32)
    vi = total[:, 4 * REC : 5 * REC]
    rq = rq / (1.0 + jnp.exp(-rq))
    low = lower[...]
    gap = 1.0 - low
    e = jnp.exp(-jnp.abs(logit))
    small, large = e / (1.0 + e), 1.0 / (1.0 + e)
    up = logit >= 0.0
    sig, neg = jnp.where(up, large, small), jnp.where(up, small, large)
    log_decay = jnp.log(low + gap * sig) + shift[...].reshape(rows, REC)
    key = gap * neg

    t, j = iota((rows, rows), 0), iota((rows, rows), 1)
    pieces = jnp.concatenate(split3(log_decay), axis=1)

    def summed(mask):
        s = nn(mask.astype(F32).astype(BF16), pieces)
        return s[:, :REC] + s[:, REC : 2 * REC] + s[:, 2 * REC :]

    cum = summed(j <= t)
    reach[...] = (rq * jnp.exp(cum)).astype(BF16)
    late = (key * jnp.exp(summed(j > t))).astype(BF16)
    state = lax.dot_general(vi, late, (((0,), (0,)), ((), ())), preferred_element_type=F32)
    chunk[rows : rows + REC] = state.astype(BF16)
    hi, mid, low3 = split3(cum[rows - 1 : rows, :])
    row = iota((DECAY_ROWS, REC), 0)
    decay = jnp.where(
        row == 0, hi.astype(F32), jnp.where(row == 1, mid.astype(F32), jnp.where(row == 2, low3.astype(F32), 0.0))
    )
    chunk[rows + REC :] = decay.astype(BF16)

    score = jnp.where(t == j, jnp.sum(rq * key, axis=1, keepdims=True), 0.0)
    h = 1
    while h < rows:
        base = t - (t & (2 * h - 1))
        mid_t = base + (h - 1)
        factor = jnp.exp(summed((j > jnp.minimum(t, mid_t)) & (j <= jnp.maximum(t, mid_t))))
        level = nt((rq * factor).astype(BF16), (key * factor).astype(BF16))
        score = jnp.where((t > mid_t) & (j >= base) & (j <= mid_t), level, score)
        h *= 2
    inner[...] = nn(score.astype(BF16), vi)


def project(ntp, xg, gain, w, lower, shift):
    rows = 2 * xg.shape[2]
    vmem = pl.BlockSpec(memory_space=pltpu.VMEM)
    return pl.pallas_call(
        functools.partial(project_kernel, ntp),
        out_shape=(
            jax.ShapeDtypeStruct((2 * rows, REC), BF16),
            jax.ShapeDtypeStruct((rows + REC + DECAY_ROWS, REC), BF16),
            jax.ShapeDtypeStruct((rows, REC), BF16),
            jax.ShapeDtypeStruct((rows, REC), F32),
        ),
        in_specs=[vmem, vmem, pl.BlockSpec(memory_space=pl.ANY), vmem, vmem],
        out_specs=(vmem,) * 4,
        scratch_shapes=[
            pltpu.VMEM((*w.shape[:3], w.shape[3] - 2 * REC), BF16),
            pltpu.SemaphoreType.DMA,
        ],
        name="project",
    )(xg, gain, w, lower, shift)


def mix_kernel(
    nz, chunk, q2, offset, reach, inner, gain, att, rec,
    buf, later, near, run, far, state_near, state_run, state_far, ring_send, ring_recv,
):
    z, _, _, up, down = place(nz)
    ways = ((up, 0, nz // 2, -1), (down, 1, nz - 1 - nz // 2, 1))
    rows = q2.shape[0] // 2
    heads = 2
    greet([up, down])

    def slot_of(d, sign):
        return (z + sign * d + nz) % nz

    def hop(way, d, j, device, sign):
        ref = buf.at[slot_of(d - 1, sign), j]
        return send(ref, ref, ring_send.at[way, d - 1, j], ring_recv.at[way, d - 1, j], device)

    def arrived(way, d, j, device, sign):
        ref = buf.at[slot_of(d, sign), j]
        send(ref, ref, ring_send.at[way, d - 1, j], ring_recv.at[way, d - 1, j], device).wait_recv()

    first = []
    for j in range(KV_PARTS):
        for device, way, count, _ in ways:
            if count > 0:
                first.append(
                    send(chunk.at[j], buf.at[z, j], ring_send.at[way, 0, j], ring_recv.at[way, 0, j], device)
                )
                first[-1].start()

    t, j = iota((rows, rows), 0), iota((rows, rows), 1)
    later[...] = (t > j).astype(F32).astype(BF16)
    state_near[...] = jnp.zeros_like(state_near)
    state_far[...] = jnp.zeros_like(state_far)
    state_run[...] = jnp.zeros_like(state_run)
    far[...] = jnp.zeros_like(far)

    def scores(h, kv, mask=None):
        s2 = nt(q2[h * rows : (h + 1) * rows], kv) * (HEAD**-0.5 * LOG2E) + offset[h] * LOG2E
        soft = jnp.log(1.0 + jnp.exp2(-jnp.abs(s2))) * LOG2E
        spent = jnp.maximum(s2, 0.0) + soft
        gain2 = jnp.minimum(s2, 0.0) - soft
        if mask is not None:
            spent = jnp.where(mask, spent, 0.0)
        hi = spent.astype(BF16)
        lo = (spent - hi.astype(F32)).astype(BF16)
        tail = nn(hi, later[...]) + nn(lo, later[...])
        return gain2 - tail, tail[:, 0:1] + spent[:, 0:1]

    flat = chunk[...].reshape(-1, REC)
    kv = flat[:rows]
    seen = j < t
    for h in range(heads):
        own = slice(h * rows, (h + 1) * rows)
        power, total = scores(h, kv, seen)
        weight = jnp.where(seen, jnp.exp2(power), 0.0).astype(BF16)
        near[own] = nn(weight, kv)
        run[own] = total

    def decay_of(block):
        rows3 = block[rows + REC : rows + REC + 8].astype(F32)
        return rows3[0:1] + rows3[1:2] + rows3[2:3]

    def use_near(d):
        @pl.when(z - d >= 0)
        def _():
            block = buf[slot_of(d, -1)].reshape(-1, REC)
            kv = block[:rows]
            for h in range(heads):
                own = slice(h * rows, (h + 1) * rows)
                power, total = scores(h, kv)
                before = run[own]
                near[own] += nn(jnp.exp2(power - before).astype(BF16), kv)
                run[own] = before + total
            before = state_run[...]
            state_near[...] += jnp.exp(before) * block[rows : rows + REC].astype(F32)
            state_run[...] = before + decay_of(block)

    def use_far(d):
        @pl.when(z + d >= nz)
        def _():
            block = buf[slot_of(d, 1)].reshape(-1, REC)
            kv = block[:rows]
            for h in range(heads):
                own = slice(h * rows, (h + 1) * rows)
                power, total = scores(h, kv)
                far[own] = far[own] * jnp.exp2(-total) + nn(jnp.exp2(power).astype(BF16), kv)
            state_far[...] = state_far[...] * jnp.exp(decay_of(block)) + block[rows : rows + REC].astype(F32)

    def forward(d, some):
        for j in range(KV_PARTS):
            for device, way, _, sign in some:
                arrived(way, d - 1, j, device, sign)
                hop(way, d, j, device, sign).start()

    def body(d, _):
        forward(d, ways)
        use_near(d - 1)
        use_far(d - 1)
        return 0

    both = min(count for _, _, count, _ in ways)
    most = ways[0][2]
    lax.fori_loop(2, both + 1, body, 0)
    for d in range(max(both + 1, 2), most + 1):
        forward(d, ways[:1])
        if d == both + 1:
            for j in range(KV_PARTS):
                arrived(1, both, j, down, 1)
            use_near(both)
            use_far(both)
        else:
            use_near(d - 1)
    for j in range(KV_PARTS):
        arrived(0, most, j, up, -1)
    use_near(most)

    lane = iota((rows, REC), 1)
    outs = []
    for h in range(heads):
        own = slice(h * rows, (h + 1) * rows)
        outs.append(near[own] + jnp.exp2(-run[own]) * far[own])
    att[...] = jnp.where(lane < HEAD, pltpu.roll(outs[0], HEAD, 1), outs[1]).astype(BF16)
    state = state_near[...] + jnp.exp(state_run[...]) * state_far[...]
    raw = inner[...] + nt(reach[...], state.astype(BF16))
    mean = jnp.sum(raw * raw, axis=1, keepdims=True) / REC
    rec[...] = (raw * lax.rsqrt(mean + EPS) * gain[...]).astype(BF16)

    for copy in first:
        copy.wait_send()

    def drain(d, _):
        for j in range(KV_PARTS):
            for device, way, _, sign in ways:
                hop(way, d, j, device, sign).wait_send()
        return 0

    lax.fori_loop(2, both + 1, drain, 0)
    for d in range(max(both + 1, 2), most + 1):
        for j in range(KV_PARTS):
            hop(0, d, j, up, -1).wait_send()


def mix(nz, chunk, q2, offset, reach, inner, gain):
    rows = reach.shape[0]
    steps = nz // 2
    dma = pltpu.SemaphoreType.DMA
    vmem = pl.BlockSpec(memory_space=pltpu.VMEM)
    chunk = chunk.reshape(KV_PARTS, -1, REC)
    return pl.pallas_call(
        functools.partial(mix_kernel, nz),
        out_shape=(
            jax.ShapeDtypeStruct((rows, REC), BF16),
            jax.ShapeDtypeStruct((rows, REC), BF16),
        ),
        in_specs=[vmem, vmem, pl.BlockSpec(memory_space=pltpu.SMEM), vmem, vmem, vmem],
        out_specs=(vmem,) * 2,
        scratch_shapes=[
            pltpu.VMEM((nz, *chunk.shape), BF16),
            pltpu.VMEM((rows, rows), BF16),
            pltpu.VMEM((2 * rows, REC), F32),
            pltpu.VMEM((2 * rows, 1), F32),
            pltpu.VMEM((2 * rows, REC), F32),
            pltpu.VMEM((REC, REC), F32),
            pltpu.VMEM((1, REC), F32),
            pltpu.VMEM((REC, REC), F32),
            dma((2, steps, KV_PARTS)), dma((2, steps, KV_PARTS)),
        ],
        compiler_params=pltpu.CompilerParams(collective_id=1, has_side_effects=True),
        name="mix",
    )(chunk, q2, offset, reach, inner, gain)


def out_kernel(
    nz, ntp, att, rec, w, out, wv, away, back, home, parts, got,
    w_sem, swap_send, swap_recv, part_send, part_recv,
):
    _, c, partner, _, _ = place(nz)
    x = lax.axis_index("tp")
    half = att.shape[0] // 2
    share = half // ntp
    copy = pltpu.make_async_copy(w.at[:, :, :, : 2 * REC], wv, w_sem)
    copy.start()
    greet([partner] + [{"tp": (x + i) % ntp} for i in range(1, ntp)])
    copy.wait()
    weights = wv[...].reshape(-1, 2 * REC)

    def partial(core):
        own = pl.ds(pl.multiple_of(half * core, half), half)
        return nt(jnp.concatenate([att[own, :], rec[own, :]], axis=1), weights)

    away[...] = partial(1 - c).astype(BF16)
    swap = send(away, back, swap_send, swap_recv, partner)
    swap.start()
    home[...] = partial(c)
    swap.wait_recv()
    total = home[...] + back[...].astype(F32)
    parts[...] = total.astype(BF16).reshape(ntp, share, -1)
    copies = []
    for i in range(1, ntp):
        copies.append(
            send(parts.at[(x + i) % ntp], got.at[i - 1], part_send.at[i - 1], part_recv.at[i - 1], {"tp": (x + i) % ntp})
        )
        copies[-1].start()
    result = parts[x].astype(F32)
    for i in range(1, ntp):
        copies[i - 1].wait_recv()
        result = result + got[i - 1].astype(F32)
    out[...] = result.astype(BF16)
    swap.wait_send()
    for copy in copies:
        copy.wait_send()


def project_out(nz, ntp, att, rec, w):
    rows = att.shape[0]
    half = rows // 2
    width = w.shape[0] * w.shape[1] * w.shape[2]
    dma = pltpu.SemaphoreType.DMA
    vmem = pl.BlockSpec(memory_space=pltpu.VMEM)
    return pl.pallas_call(
        functools.partial(out_kernel, nz, ntp),
        out_shape=jax.ShapeDtypeStruct((half // ntp, width), BF16),
        in_specs=[vmem, vmem, pl.BlockSpec(memory_space=pl.ANY)],
        out_specs=vmem,
        scratch_shapes=[
            pltpu.VMEM((*w.shape[:3], 2 * REC), BF16),
            pltpu.VMEM((half, width), BF16),
            pltpu.VMEM((half, width), BF16),
            pltpu.VMEM((half, width), F32),
            pltpu.VMEM((ntp, half // ntp, width), BF16),
            pltpu.VMEM((ntp - 1, half // ntp, width), BF16),
            dma, dma, dma, dma((ntp - 1,)), dma((ntp - 1,)),
        ],
        compiler_params=pltpu.CompilerParams(collective_id=2, has_side_effects=True),
        name="project_out",
    )(att, rec, w)


def on_device(
    nz,
    ntp,
    tokens,
    norm_gain,
    att_q_weight,
    att_k_weight,
    att_v_weight,
    rec_q_weight,
    rec_f_weight,
    rec_i_weight,
    att_out_weight,
    rec_out_weight,
    score_offset,
    lower_bound,
    decay_shift,
    rec_gain,
):
    c = lax.axis_index("sp") % 2

    def halves(weight):
        return weight.reshape(2, weight.shape[0] // 2, weight.shape[1])

    wt = jnp.concatenate(
        [
            halves(weight)
            for weight in (
                att_out_weight,
                rec_out_weight,
                att_q_weight,
                att_k_weight,
                att_v_weight,
                rec_q_weight,
                rec_f_weight,
                rec_i_weight,
            )
        ],
        axis=1,
    ).transpose(0, 2, 1)
    wt = wt.reshape(2, PARTS // 2, -1, wt.shape[2])
    xg, w, shift = gather(nz, ntp, tokens, wt, decay_shift)
    lower = lax.dynamic_index_in_dim(lower_bound.reshape(2, 1, REC), c, 0, keepdims=False)
    gain = lax.dynamic_index_in_dim(rec_gain.reshape(2, 1, REC), c, 0, keepdims=False)
    offset = lax.dynamic_index_in_dim(score_offset.reshape(2, 2), c, 0, keepdims=False)
    q2, chunk, reach, inner = project(ntp, xg, norm_gain.reshape(1, -1), w, lower, shift)
    att, rec = mix(nz, chunk, q2, offset, reach, inner, gain)
    return project_out(nz, ntp, att, rec, w)


def solution(mesh):
    in_specs = (
        P(("grp", "sp"), "tp"),
        P(),
        P("tp", "sp"),
        P("tp", "sp"),
        P("tp", "sp"),
        P("tp", "sp"),
        P("tp", "sp"),
        P("tp", "sp"),
        P("tp", "sp"),
        P("tp", "sp"),
        P("tp"),
        P("tp"),
        P(("grp", "sp"), "tp"),
        P("tp"),
    )
    out_specs = P(("grp", "sp", "tp"), None)
    return jax.shard_map(
        functools.partial(on_device, mesh.shape["sp"] // 2, mesh.shape["tp"]),
        mesh=mesh,
        in_specs=in_specs,
        out_specs=out_specs,
        check_vma=False,
    )
```

time: 573 us -> 201 us (0.35)
  the two profiles are of different devices: /device:TPU:1824 before, /device:TPU:33 now
where the time goes in v1:
time: 201 us
  Pallas kernels  192 us (96%)
  local copies, waits for them, and re-layouts  8.56 us (4%)
    pallas_call x1, Pallas kernels, gather(): pl.pallas_call(functools.partial(gather_kernel, nz, ntp), out_shape=(jax....  99.1 us
    pallas_call x1, Pallas kernels, mix(): pl.pallas_call(functools.partial(mix_kernel, nz), out_shape=(jax.ShapeDty...  55 us
    pallas_call x1, Pallas kernels, project_out(): pl.pallas_call(functools.partial(out_kernel, nz, ntp), out_shape=jax.Shap...  30.2 us
    pallas_call x1, Pallas kernels, project(): pl.pallas_call(functools.partial(project_kernel, ntp), out_shape=(jax.Sha...  7.71 us

profile of v1, /device:TPU:33, one launch (start us, length us, event | category | flops | bytes accessed | tf_op | source)
XLA Modules:
  0.0 200.6 jit_solution(16028154551629964813)
XLA Ops:
  0.0 0.0 copy-start
  0.0 0.7 reshape.54
  0.8 0.5 fusion.1.offset
  1.3 1.2 fusion
  2.5 0.8 reshape.45
  3.3 0.8 reshape.46
  4.1 0.0 copy-done
  4.1 0.7 copy_bitcast_fusion.2
  4.8 0.7 copy_bitcast_fusion
  5.5 0.7 copy_bitcast_fusion.4
  6.3 0.7 concatenate.3
  7.0 99.1 %gather_weights.1 = (bf16[4,2,128,512]{3,2,1,0:T(8,128)(2,1)}, bf16[32,4,16,896]{3,2,1,0:T(8,128)(2,1)}, f32[2,128,128]{2,1,0:T(8,128)}) custom-call(bf16[128,512]{1,0:T(8,128)(2,1)} %tok.1, bf16[2,2,16,896]{3,2,1,0:T(8,128)(2,1)} %bitcast.47, f32[128,256]{1,0:T(8,128)} %shift.1), custom_call_target="tpu_custom_call" | custom-call | tf_op jit(solution)/shard_map/gather_weights/pallas_call | solution.py:180
  106.1 7.7 %project.1 = (bf16[512,128]{1,0:T(8,128)(2,1)}, bf16[400,128]{1,0:T(8,128)(2,1)}, bf16[256,128]{1,0:T(8,128)(2,1)}, f32[256,128]{1,0:T(8,128)}) custom-call(bf16[4,2,128,512]{3,2,1,0:T(8,128)(2,1)} %get-tuple-element.14.xg, f32[1,2048]{1,0:T(1,128)} %bitcast.49, bf16[32,4,16,896]{3,2,1,0:T(8,128)(2,1)} %get-tuple-element.15.w, ...), custom_call_target="tpu_custom_call" | custom-call | tf_op jit(solution)/shard_map/project/pallas_call | solution.py:283
  113.9 55.0 %mix.1 = (bf16[256,128]{1,0:T(8,128)(2,1)}, bf16[256,128]{1,0:T(8,128)(2,1)}) custom-call(bf16[5,80,128]{2,1,0:T(8,128)(2,1)} %bitcast.48, bf16[512,128]{1,0:T(8,128)(2,1)} %get-tuple-element.18.q2, f32[2]{0:T(128)} %fusion.1.offset, bf16[256,128]{1,0:T(8,128)(2,1)} %get-tuple-element.19.reach, f32[256,128]{1,0:T(8,128)} %get-tuple-element.20.inner, ...), custom_call_target="tpu_custom_call" | custom-call | tf_op jit(solution)/shard_map/mix/pallas_call | solution.py:450
  168.9 30.2 %project_out.1 = bf16[32,2048]{1,0:T(8,128)(2,1)} custom-call(bf16[256,128]{1,0:T(8,128)(2,1)} %get-tuple-element.21.att, bf16[256,128]{1,0:T(8,128)(2,1)} %get-tuple-element.22.rec, bf16[32,4,16,896]{3,2,1,0:T(8,128)(2,1)} %get-tuple-element.15.w), custom_call_target="tpu_custom_call" | custom-call | tf_op jit(solution)/shard_map/project_out/pallas_call | solution.py:521
  199.1 1.6 copy.36
  (2 shorter events, 0.0 us)
Async XLA Ops:
  0.0 4.1 %copy-start = (bf16[256,32]{0,1:T(8,128)(2,1)S(1)}, bf16[256,32]{0,1:T(8,128)(2,1)}, u32[]{:S(2)}) copy-start(bf16[256,32]{0,1:T(8,128)(2,1)} %param.16) | copy-start | bytes 49156
